TPU v7x, 32 devices: a whole 2x2x4 slice. The times are simulated.
32 devices in a mesh: rep: 4 (over z), fs: 4 (over y, x), tp: 2 (over core).
Axes of the slice: x: 2, y: 2, z: 4, core: 2. Of those that a mesh axis runs over, the one named last changes fastest.
Arguments:
- tokens_in: bfloat16 [3072, 1024], P(('rep', 'fs', 'tp')), may hold values from -6 to 6
- out_grad: bfloat16 [3072, 1024], P(('rep', 'fs', 'tp')), may hold values from -6 to 6
- gate_weight: bfloat16 [1024, 2816], P('fs', 'tp'), may hold values from -0.1875 to 0.1875
- up_weight: bfloat16 [1024, 2816], P('fs', 'tp'), may hold values from -0.1875 to 0.1875
- down_weight: bfloat16 [2816, 1024], P('tp', 'fs'), may hold values from -0.109375 to 0.109375
Outputs:
- grad_in: bfloat16 [3072, 1024], P(('rep', 'fs', 'tp'))
- grad_gate_w: float32 [1024, 2816], P('fs', 'tp')
- grad_up_w: float32 [1024, 2816], P('fs', 'tp')
- grad_down_w: float32 [2816, 1024], P('tp', 'fs')
All inputs are finite; a program needn't handle non-finite values.
Results may differ from a plain program's by a relative error of at most 0.02.
Values may be sent and summed in bfloat16 or wider, within the bound.
A program may use at most 64 MiB of HBM per device.

v0:
```python
import jax
import jax.numpy as jnp
from jax import lax
from jax.sharding import PartitionSpec as P


def contract_last(left, right):
    return lax.dot_general(
        left, right, (((1,), (1,)), ((), ())), preferred_element_type=jnp.float32
    )


def contract_first(left, right):
    return lax.dot_general(
        left, right, (((0,), (0,)), ((), ())), preferred_element_type=jnp.float32
    )


def body(tokens_in, out_grad, gate_weight, up_weight, down_weight):
    replicas = lax.axis_size("rep")
    shards = lax.axis_size("fs")
    columns = lax.axis_size("tp")
    local_rows = tokens_in.shape[0]
    hidden_cols = gate_weight.shape[1]
    factor = (local_rows * replicas * shards * columns) ** (-0.5)
    part = hidden_cols // replicas
    offset = lax.axis_index("rep") * part
    pieces = jnp.stack(
        [
            lax.dynamic_slice_in_dim(gate_weight, offset, part, 1).T,
            lax.dynamic_slice_in_dim(up_weight, offset, part, 1).T,
            lax.dynamic_slice_in_dim(down_weight, offset, part, 0),
        ]
    )
    full = lax.all_gather(pieces, "fs", axis=2, tiled=True)
    gate_full, up_full, down_full = (full[0], full[1], full[2])
    both = lax.all_gather(jnp.stack([tokens_in, out_grad]), ("rep", "tp"), axis=1, tiled=True)
    tokens_all, grads_all = (both[0], both[1])
    gate = contract_last(tokens_all, gate_full).astype(jnp.bfloat16)
    up_proj = contract_last(tokens_all, up_full).astype(jnp.bfloat16)
    gate_wide = gate.astype(jnp.float32)
    up_wide = up_proj.astype(jnp.float32)
    sigmoid = jax.nn.sigmoid(gate_wide)
    activated = gate_wide * sigmoid
    hidden = (activated * up_wide).astype(jnp.bfloat16)
    grad_hidden = contract_last(grads_all, down_full).astype(jnp.bfloat16)
    grad_wide = grad_hidden.astype(jnp.float32)
    grad_gate = (grad_wide * up_wide * sigmoid * (1.0 + gate_wide * (1.0 - sigmoid))).astype(
        jnp.bfloat16
    )
    grad_up = (grad_wide * activated).astype(jnp.bfloat16)
    weights = factor * jnp.stack(
        [
            contract_first(grad_gate, tokens_all),
            contract_first(grad_up, tokens_all),
            contract_first(hidden, grads_all),
        ]
    )
    owned = lax.psum_scatter(weights.astype(jnp.bfloat16), "fs", scatter_dimension=2, tiled=True)
    summed = lax.all_gather(owned, "rep", axis=1, tiled=True).astype(jnp.float32)
    partial = jnp.dot(grad_gate, gate_full, preferred_element_type=jnp.float32) + jnp.dot(
        grad_up, up_full, preferred_element_type=jnp.float32
    )
    grad_in = lax.psum_scatter(
        partial.astype(jnp.bfloat16), ("rep", "tp"), scatter_dimension=0, tiled=True
    )
    return (grad_in, summed[0].T, summed[1].T, summed[2])


def solution(mesh):
    placed = (
        P(("rep", "fs", "tp"), None),
        P(("rep", "fs", "tp"), None),
        P("fs", "tp"),
        P("fs", "tp"),
        P("tp", "fs"),
    )
    return jax.shard_map(
        body,
        mesh=mesh,
        in_specs=placed,
        out_specs=(P(("rep", "fs", "tp"), None), P("fs", "tp"), P("fs", "tp"), P("tp", "fs")),
        check_vma=False,
    )
```

profile of v0, /device:TPU:0, one launch (start us, length us, event | category | flops | bytes accessed | tf_op | source)
XLA Modules:
  0.0 225.2 jit_solution(11727370553388090820)
XLA Ops:
  7.2 1.0 copy-done
  8.3 1.3 constant_dynamic-slice_fusion
  9.6 0.1 copy.16
  9.8 0.1 copy.15
  9.9 0.9 pad_maximum_fusion
  10.9 0.8 pad_maximum_fusion.1
  11.7 37.5 %all-gather.6.cloned.1.call-done = bf16[3,352,1024]{2,1,0:T(8,128)(2,1)} async-done(((bf16[3,352,256]{2,1,0:T(8,128)(2,1)}), bf16[3,352,1024]{2,1,0:T(8,128)(2,1)}) %all-gather.6.cloned.1.call-update) | async-done | bytes 2162704 | tf_op jit(solution)/shard_map/all_gather | solution.py:35
  49.2 40.4 %all-gather.4.cloned.1.call-done = bf16[2,768,1024]{2,1,0:T(8,128)(2,1)} async-done(((bf16[2,96,1024]{2,1,0:T(8,128)(2,1)}), bf16[2,768,1024]{2,1,0:T(8,128)(2,1)}) %all-gather.4.cloned.1.call-update) | async-done | bytes 3145744 | tf_op jit(solution)/shard_map/all_gather | solution.py:37
  89.7 2.5 %convolution_convert_fusion.1 = bf16[768,352]{0,1:T(8,128)(2,1)S(1)} fusion(bf16[2,768,1024]{2,1,0:T(8,128)(2,1)} %all-gather.4.cloned.1.call-done, bf16[3,352,1024]{2,1,0:T(8,128)(2,1)} %all-gather.6.cloned.1.call-done), kind=kOutput, calls=%fused_computation.20 | convolution fusion | flops 553918464 | bytes 2834432 | tf_op jit(solution)/shard_map/dot_general | solution.py:8
  92.3 2.2 fusion.2
  94.4 0.8 convolution_convert_fusion
  95.2 0.8 convolution_bitcast_fusion
  96.1 0.9 convolution_bitcast_fusion.1
  96.9 1.0 convolution_bitcast_fusion.2
  98.0 2.0 fusion
  100.0 34.8 %reduce-scatter.5.cloned.1.call-done = bf16[3,352,256]{2,1,0:T(8,128)(2,1)} async-done(((bf16[3,352,1024]{2,1,0:T(8,128)(2,1)}), bf16[3,352,256]{2,1,0:T(8,128)(2,1)}) %reduce-scatter.5.cloned.1.call-update) | async-done | bytes 540688 | tf_op jit(solution)/shard_map/reduce_scatter | solution.py:59
  134.8 2.5 %fusion.12 = f32[768,1024]{1,0:T(8,128)S(1)} fusion(bf16[3,352,1024]{2,1,0:T(8,128)(2,1)S(1)} %copy-done.4, bf16[768,352]{0,1:T(8,128)(2,1)} %copy-done.7, bf16[768,352]{0,1:T(8,128)(2,1)S(1)} %fusion.2, bf16[768,352]{0,1:T(8,128)(2,1)} %copy-done.5), kind=kOutput, calls=%fused_computation.33 | convolution fusion | flops 557162496 | bytes 5488640 | tf_op jit(solution)/shard_map/dot_general | solution.py:61
  137.4 2.3 %add_convert_fusion = bf16[768,1024]{1,0:T(8,128)(2,1)} fusion(f32[768,1024]{1,0:T(8,128)S(1)} %fusion.12, bf16[3,352,1024]{2,1,0:T(8,128)(2,1)S(1)} %copy-done.4, bf16[768,352]{0,1:T(8,128)(2,1)S(1)} %fusion.2, bf16[768,352]{0,1:T(8,128)(2,1)S(1)} %copy-done.6), kind=kOutput, calls=%fused_computation.2 | convolution fusion | flops 557383680 | bytes 6520832 | tf_op jit(solution)/shard_map/dot_general | solution.py:61
  139.7 43.2 %all-gather.8.cloned.1.call-done = bf16[3,1408,256]{2,1,0:T(8,128)(2,1)} async-done(((bf16[3,352,256]{2,1,0:T(8,128)(2,1)}), bf16[3,1408,256]{2,1,0:T(8,128)(2,1)}) %all-gather.8.cloned.1.call-update) | async-done | bytes 2162704 | tf_op jit(solution)/shard_map/all_gather | solution.py:60
  183.0 2.0 convert_element_type.47
  185.0 2.0 slice_bitcast_fusion.2
  186.9 2.9 %copy.13 = f32[256,1408]{1,0:T(8,128)} copy(f32[256,1408]{0,1:T(8,128)} %get-tuple-element.14) | data formatting | bytes 2883584
  189.8 1.5 copy.14
  191.4 27.3 %reduce-scatter.3.cloned.1.call-done = bf16[96,1024]{1,0:T(8,128)(2,1)} async-done(((bf16[768,1024]{1,0:T(8,128)(2,1)}), bf16[96,1024]{1,0:T(8,128)(2,1)}) %reduce-scatter.3.cloned.1.call-update) | async-done | bytes 196624 | tf_op jit(solution)/shard_map/reduce_scatter | solution.py:64
  (26 shorter events, 0.4 us)
Async XLA Ops:
  7.2 1.1 copy-start
  7.2 42.1 %all-gather.6.cloned.1.call-start = ((), (), s32[]{:S(2)}) async-start(), calls=%async_computation.3 | async-start | bytes 2703360 | tf_op jit(solution)/shard_map/all_gather | solution.py:35
  8.3 2.5 %copy-start.1 = (bf16[96,1024]{1,0:T(8,128)(2,1)S(1)}, bf16[96,1024]{1,0:T(8,128)(2,1)}, u32[]{:S(2)}) copy-start(bf16[96,1024]{1,0:T(8,128)(2,1)} %param.6) | copy-start | bytes 589828
  8.3 2.5 %copy-start.2 = (bf16[96,1024]{1,0:T(8,128)(2,1)S(1)}, bf16[96,1024]{1,0:T(8,128)(2,1)}, u32[]{:S(2)}) copy-start(bf16[96,1024]{1,0:T(8,128)(2,1)} %param.5) | copy-start | bytes 589828
  10.8 78.9 %all-gather.4.cloned.1.call-start = ((), (), s32[]{:S(2)}) async-start(), calls=%async_computation.2 | async-start | bytes 3538944 | tf_op jit(solution)/shard_map/all_gather | solution.py:37
  11.7 123.1 %reduce-scatter.5.cloned.1.call-start = ((), (), s32[]{:S(2)}) async-start(), calls=%async_computation.5 | async-start | bytes 2703360 | tf_op jit(solution)/shard_map/reduce_scatter | solution.py:59
  89.7 2.6 %copy-start.3 = (bf16[2,768,1024]{2,1,0:T(8,128)(2,1)S(1)}, bf16[2,768,1024]{2,1,0:T(8,128)(2,1)}, u32[]{:S(2)}) copy-start(bf16[2,768,1024]{2,1,0:T(8,128)(2,1)} %all-gather.4.cloned.1.call-done) | copy-start | bytes 9437188
  92.2 4.7 %copy-start.7 = (bf16[768,352]{0,1:T(8,128)(2,1)}, bf16[768,352]{0,1:T(8,128)(2,1)S(1)}, u32[]{:S(2)}) copy-start(bf16[768,352]{0,1:T(8,128)(2,1)S(1)} %convolution_convert_fusion.1) | copy-start | bytes 1622020
  92.2 2.2 copy-start.4
  95.2 1.7 copy-start.5
  100.0 83.0 %all-gather.8.cloned.1.call-start = ((), (), s32[]{:S(2)}) async-start(), calls=%async_computation.6 | async-start | bytes 2703360 | tf_op jit(solution)/shard_map/all_gather | solution.py:60
  134.8 83.8 %reduce-scatter.3.cloned.1.call-start = ((), (), s32[]{:S(2)}) async-start(), calls=%async_computation.4 | async-start | bytes 1769472 | tf_op jit(solution)/shard_map/reduce_scatter | solution.py:64
  134.8 2.6 %copy-start.6 = (bf16[768,352]{0,1:T(8,128)(2,1)S(1)}, bf16[768,352]{0,1:T(8,128)(2,1)}, u32[]{:S(2)}) copy-start(bf16[768,352]{0,1:T(8,128)(2,1)} %copy-done.5) | copy-start | bytes 1622020
Sparse Core Ops, SparseCore 0:
  10.9 38.2 all-gather.5
  51.4 38.1 all-gather.3
  100.1 34.6 reduce-scatter.4
  136.2 46.7 all-gather.7
  185.7 32.8 reduce-scatter.2
where the time goes:
time: 225 us
  waiting for transfers between devices  183 us (81%)
  between operations  13.9 us (6%)
  matrix products  13 us (6%)
  local copies, waits for them, and re-layouts  9.14 us (4%)
  other arithmetic  5.58 us (2%)
    all_gather x1, waiting for transfers between devices, body(): lax.all_gather(owned, 'rep', axis=1, tiled=True).astype(jnp.float32)  43.2 us
    all_gather x1, waiting for transfers between devices, body(): lax.all_gather(jnp.stack([tokens_in, out_grad]), ('rep', 'tp'), axis=1, t...  40.4 us
    all_gather x1, waiting for transfers between devices, body(): full = lax.all_gather(pieces, 'fs', axis=2, tiled=True)  37.5 us
    reduce_scatter x1, waiting for transfers between devices, body(): lax.psum_scatter(weights.astype(jnp.bfloat16), 'fs', scatter_dimension=2,...  34.8 us
    reduce_scatter x1, waiting for transfers between devices, body(): lax.psum_scatter(partial.astype(jnp.bfloat16), ('rep', 'tp'), scatter_dim...  27.3 us
    unnamed x20, local copies, waits for them, and re-layouts  5.87 us
    dot_general x3, matrix products, contract_last(): lax.dot_general(left, right, (((1,), (1,)), ((), ())), preferred_element_...  5.44 us
  transfers between devices with their start and end apart: 5, of which 5 were waited for; matrix products, arithmetic and copies ran while one was open for 6% of the time, Pallas kernels for 0%

commit v1 on v0

--- a/solution.py
+++ b/solution.py
@@ -32,7 +32,7 @@
             lax.dynamic_slice_in_dim(down_weight, offset, part, 0),
         ]
     )
-    full = lax.all_gather(pieces, "fs", axis=2, tiled=True)
+    full = jnp.concatenate(lax.all_gather(pieces, "fs"), axis=2)
     gate_full, up_full, down_full = (full[0], full[1], full[2])
     both = lax.all_gather(jnp.stack([tokens_in, out_grad]), ("rep", "tp"), axis=1, tiled=True)
     tokens_all, grads_all = (both[0], both[1])

time: 225 us -> 224 us (level)
  local copies, waits for them, and re-layouts: 9.14 us -> 13.5 us
  waiting for transfers between devices: 183 us -> 179 us
    all_gather x1, waiting for transfers between devices: 40.4 us -> 36 us  [body(): lax.all_gather(jnp.stack([tokens_in, out_grad]), ('rep', 'tp'), axis=1, t...]
    all_gather x0 -> x1, local copies, waits for them, and re-layouts: none -> 3.28 us  [body(): full = jnp.concatenate(lax.all_gather(pieces, 'fs'), axis=2)]
    unnamed x20 -> x17, local copies, waits for them, and re-layouts: 5.87 us -> 6.2 us
  transfers between devices with their start and end apart: 5 -> 5, of which waited for: 5 -> 5; matrix products, arithmetic and copies ran while one was open for 6% -> 8% of each run, Pallas kernels for 0% -> 0%
where the time goes in v1:
time: 224 us
  waiting for transfers between devices  179 us (80%)
  between operations  14 us (6%)
  local copies, waits for them, and re-layouts  13.5 us (6%)
  matrix products  11.2 us (5%)
  other arithmetic  5.58 us (2%)
    all_gather x1, waiting for transfers between devices, body(): lax.all_gather(owned, 'rep', axis=1, tiled=True).astype(jnp.float32)  43.5 us
    all_gather x1, waiting for transfers between devices, body(): full = jnp.concatenate(lax.all_gather(pieces, 'fs'), axis=2)  37.7 us
    all_gather x1, waiting for transfers between devices, body(): lax.all_gather(jnp.stack([tokens_in, out_grad]), ('rep', 'tp'), axis=1, t...  36 us
    reduce_scatter x1, waiting for transfers between devices, body(): lax.psum_scatter(weights.astype(jnp.bfloat16), 'fs', scatter_dimension=2,...  34.7 us
    reduce_scatter x1, waiting for transfers between devices, body(): lax.psum_scatter(partial.astype(jnp.bfloat16), ('rep', 'tp'), scatter_dim...  27.3 us
    unnamed x17, local copies, waits for them, and re-layouts  6.2 us
  transfers between devices with their start and end apart: 5, of which 5 were waited for; matrix products, arithmetic and copies ran while one was open for 8% of the time, Pallas kernels for 0%

profile of v1, /device:TPU:0, one launch (start us, length us, event | category | flops | bytes accessed | tf_op | source)
XLA Modules:
  0.0 223.7 jit_solution(18158454545901701577)
XLA Ops:
  7.2 1.0 copy-done
  8.3 1.3 constant_dynamic-slice_fusion
  9.9 0.9 pad_maximum_fusion
  10.9 0.8 pad_maximum_fusion.1
  11.7 37.7 %all-gather.9.cloned.1.call-done = bf16[12,352,256]{2,1,0:T(8,128)(2,1)} async-done(((bf16[3,352,256]{2,1,0:T(8,128)(2,1)}), bf16[12,352,256]{2,1,0:T(8,128)(2,1)}) %all-gather.9.cloned.1.call-update) | async-done | bytes 2162704 | tf_op jit(solution)/shard_map/all_gather | solution.py:35
  49.4 3.3 %copy.31 = bf16[4,3,352,256]{3,0,2,1:T(4,128)(2,1)S(1)} copy(bf16[4,3,352,256]{3,2,1,0:T(8,128)(2,1)} %bitcast.60) | data formatting | bytes 4325376 | tf_op jit(solution)/shard_map/all_gather | solution.py:35
  52.7 0.7 fusion.19
  53.8 36.0 %all-gather.5.cloned.1.call-done = bf16[2,768,1024]{2,1,0:T(8,128)(2,1)} async-done(((bf16[2,96,1024]{2,1,0:T(8,128)(2,1)}), bf16[2,768,1024]{2,1,0:T(8,128)(2,1)}) %all-gather.5.cloned.1.call-update) | async-done | bytes 3145744 | tf_op jit(solution)/shard_map/all_gather | solution.py:37
  89.8 2.3 %convolution_convert_fusion.1 = bf16[768,352]{0,1:T(8,128)(2,1)S(1)} fusion(bf16[352,1024]{1,0:T(8,128)(2,1)S(1)} %bitcast.61, bf16[2,768,1024]{2,1,0:T(8,128)(2,1)} %all-gather.5.cloned.1.call-done), kind=kOutput, calls=%fused_computation.21 | convolution fusion | flops 553918464 | bytes 2834432 | tf_op jit(solution)/shard_map/dot_general | solution.py:8
  92.2 0.8 fusion.2
  93.0 0.8 convolution_convert_fusion
  93.8 0.8 convolution_bitcast_fusion
  94.6 0.9 convolution_bitcast_fusion.1
  95.5 1.0 convolution_bitcast_fusion.2
  96.5 2.0 fusion
  98.6 34.7 %reduce-scatter.5.cloned.1.call-done = bf16[3,352,256]{2,1,0:T(8,128)(2,1)} async-done(((bf16[3,352,1024]{2,1,0:T(8,128)(2,1)}), bf16[3,352,256]{2,1,0:T(8,128)(2,1)}) %reduce-scatter.5.cloned.1.call-update) | async-done | bytes 540688 | tf_op jit(solution)/shard_map/reduce_scatter | solution.py:59
  133.4 2.3 %fusion.17 = f32[768,1024]{1,0:T(8,128)S(1)} fusion(bf16[352,1024]{1,0:T(8,128)(2,1)S(1)} %bitcast.64, bf16[768,352]{0,1:T(8,128)(2,1)} %copy-done.4, bf16[768,352]{0,1:T(8,128)(2,1)S(1)} %fusion.2, bf16[768,352]{0,1:T(8,128)(2,1)S(1)} %convolution_convert_fusion), kind=kOutput, calls=%fused_computation.37 | convolution fusion | flops 557162496 | bytes 5488640 | tf_op jit(solution)/shard_map/dot_general | solution.py:61
  135.7 2.3 %add_convert_fusion = bf16[768,1024]{1,0:T(8,128)(2,1)} fusion(f32[768,1024]{1,0:T(8,128)S(1)} %fusion.17, bf16[352,1024]{1,0:T(8,128)(2,1)S(1)} %bitcast.62, bf16[768,352]{0,1:T(8,128)(2,1)S(1)} %fusion.2, bf16[768,352]{0,1:T(8,128)(2,1)S(1)} %convolution_convert_fusion), kind=kOutput, calls=%fused_computation.2 | convolution fusion | flops 557383680 | bytes 6520832 | tf_op jit(solution)/shard_map/dot_general | solution.py:61
  138.0 43.5 %all-gather.7.cloned.1.call-done = bf16[3,1408,256]{2,1,0:T(8,128)(2,1)} async-done(((bf16[3,352,256]{2,1,0:T(8,128)(2,1)}), bf16[3,1408,256]{2,1,0:T(8,128)(2,1)}) %all-gather.7.cloned.1.call-update) | async-done | bytes 2162704 | tf_op jit(solution)/shard_map/all_gather | solution.py:60
  181.5 2.0 convert_element_type.47
  183.5 2.0 slice_bitcast_fusion.2
  185.4 2.9 %copy.23 = f32[256,1408]{1,0:T(8,128)} copy(f32[256,1408]{0,1:T(8,128)} %get-tuple-element.22) | data formatting | bytes 2883584
  188.3 1.5 copy.24
  189.9 27.3 %reduce-scatter.3.cloned.1.call-done = bf16[96,1024]{1,0:T(8,128)(2,1)} async-done(((bf16[768,1024]{1,0:T(8,128)(2,1)}), bf16[96,1024]{1,0:T(8,128)(2,1)}) %reduce-scatter.3.cloned.1.call-update) | async-done | bytes 196624 | tf_op jit(solution)/shard_map/reduce_scatter | solution.py:64
  (25 shorter events, 1.0 us)
Async XLA Ops:
  7.2 1.1 copy-start
  7.2 42.2 %all-gather.9.cloned.1.call-start = ((), (), s32[]{:S(2)}) async-start(), calls=%async_computation.6 | async-start | bytes 2703360 | tf_op jit(solution)/shard_map/all_gather | solution.py:35
  8.3 2.5 %copy-start.1 = (bf16[96,1024]{1,0:T(8,128)(2,1)S(1)}, bf16[96,1024]{1,0:T(8,128)(2,1)}, u32[]{:S(2)}) copy-start(bf16[96,1024]{1,0:T(8,128)(2,1)} %param.6) | copy-start | bytes 589828
  8.3 2.5 %copy-start.2 = (bf16[96,1024]{1,0:T(8,128)(2,1)S(1)}, bf16[96,1024]{1,0:T(8,128)(2,1)}, u32[]{:S(2)}) copy-start(bf16[96,1024]{1,0:T(8,128)(2,1)} %param.5) | copy-start | bytes 589828
  10.8 79.0 %all-gather.5.cloned.1.call-start = ((), (), s32[]{:S(2)}) async-start(), calls=%async_computation.2 | async-start | bytes 3538944 | tf_op jit(solution)/shard_map/all_gather | solution.py:37
  11.7 121.6 %reduce-scatter.5.cloned.1.call-start = ((), (), s32[]{:S(2)}) async-start(), calls=%async_computation.4 | async-start | bytes 2703360 | tf_op jit(solution)/shard_map/reduce_scatter | solution.py:59
  89.8 2.4 %copy-start.3 = (bf16[2,768,1024]{2,1,0:T(8,128)(2,1)S(1)}, bf16[2,768,1024]{2,1,0:T(8,128)(2,1)}, u32[]{:S(2)}) copy-start(bf16[2,768,1024]{2,1,0:T(8,128)(2,1)} %all-gather.5.cloned.1.call-done) | copy-start | bytes 9437188
  92.1 3.3 %copy-start.4 = (bf16[768,352]{0,1:T(8,128)(2,1)}, bf16[768,352]{0,1:T(8,128)(2,1)S(1)}, u32[]{:S(2)}) copy-start(bf16[768,352]{0,1:T(8,128)(2,1)S(1)} %convolution_convert_fusion.1) | copy-start | bytes 1622020
  98.5 83.0 %all-gather.7.cloned.1.call-start = ((), (), s32[]{:S(2)}) async-start(), calls=%async_computation.5 | async-start | bytes 2703360 | tf_op jit(solution)/shard_map/all_gather | solution.py:60
  133.3 83.9 %reduce-scatter.3.cloned.1.call-start = ((), (), s32[]{:S(2)}) async-start(), calls=%async_computation.3 | async-start | bytes 1769472 | tf_op jit(solution)/shard_map/reduce_scatter | solution.py:64
Sparse Core Ops, SparseCore 0:
  10.9 38.4 all-gather.8
  51.6 38.1 all-gather.4
  98.6 34.6 reduce-scatter.4
  134.7 46.7 all-gather.6
  184.2 32.9 reduce-scatter.2
